TPU v7x, 32 devices: a whole 2x2x4 slice. The times are simulated.
32 devices in a mesh: fs: 8 (over z, y), tp: 4 (over x, core).
Axes of the slice: x: 2, y: 2, z: 4, core: 2. Of those that a mesh axis runs over, the one named last changes fastest.
Arguments:
- tokens: bfloat16 [8192, 2048], P('fs', 'tp'), may hold values from -6 to 6
- norm_gain: float32 [2048], P('fs'), may hold values from 0.1 to 1.9
- up_master: float32 [2048, 8192], P('fs', 'tp'), may hold values from -0.125 to 0.125
- down_master: float32 [2048, 8192], P('fs', 'tp'), may hold values from -0.0625 to 0.0625
Outputs:
- up_weights: bfloat16 [2048, 8192], P(None, 'tp')
- down_weights: bfloat16 [8192, 2048], P('tp')
- mlp_out: bfloat16 [8192, 2048], P('fs', 'tp')
All inputs are finite; a program needn't handle non-finite values.
Results may differ from a plain program's by a relative error of at most 0.014.
Values may be sent and summed in bfloat16 or wider, within the bound.
A program may use at most 128 MiB of HBM per device.

v0:
```python
import jax
import jax.numpy as jnp
from jax import lax
from jax.sharding import PartitionSpec as P

norm_floor = 1e-06


def on_device(tokens, norm_gain, up_master, down_master):
    up_local = (norm_gain[:, None] * up_master).astype(jnp.bfloat16)
    down_local = down_master.astype(jnp.bfloat16)
    gathered = lax.all_gather(tokens, "tp", axis=1, tiled=True)
    widened = gathered.astype(jnp.float32)
    normed = (
        widened * lax.rsqrt(jnp.mean(widened * widened, axis=-1, keepdims=True) + norm_floor)
    ).astype(jnp.bfloat16)
    up_whole, down_whole = (
        lax.all_gather(up_local, "fs", axis=0, tiled=True),
        lax.all_gather(down_local, "fs", axis=0, tiled=True),
    )
    preact = jnp.dot(normed, up_whole, preferred_element_type=jnp.float32)
    hidden = jnp.square(jax.nn.relu(preact)).astype(jnp.bfloat16)
    partial_value = jnp.einsum("tf,df->td", hidden, down_whole, preferred_element_type=jnp.float32)
    summed = lax.psum_scatter(
        partial_value.astype(jnp.bfloat16), "tp", scatter_dimension=1, tiled=True
    )
    return (up_whole, jnp.transpose(down_whole), summed)


def solution(mesh):
    in_specs = (P("fs", "tp"), P("fs"), P("fs", "tp"), P("fs", "tp"))
    out_specs = (P(None, "tp"), P("tp", None), P("fs", "tp"))
    return jax.shard_map(
        on_device, mesh=mesh, in_specs=in_specs, out_specs=out_specs, check_vma=False
    )
```

profile of v0, /device:TPU:0, one launch (start us, length us, event | category | flops | bytes accessed | tf_op | source)
XLA Modules:
  0.0 391.6 jit_solution(10137496696475460250)
XLA Ops:
  7.2 0.0 all-gather.8.cloned.1.call-start
  7.2 0.7 all-gather.8.cloned.1.call-update
  7.9 0.0 all-gather.4.cloned.1.call-start
  7.9 2.7 multiply_convert_fusion.1
  10.7 0.0 all-gather.4.cloned.1.call-update
  10.7 0.0 all-gather.6.cloned.1.call-start
  10.8 2.5 copy.7
  13.3 0.0 all-gather.6.cloned.1.call-update
  13.3 0.0 reduce-scatter.2.cloned.1.call-start
  13.4 33.4 %all-gather.8.cloned.1.call-done = bf16[1024,2048]{1,0:T(8,128)(2,1)} async-done(((bf16[1024,512]{1,0:T(8,128)(2,1)}), bf16[1024,2048]{1,0:T(8,128)(2,1)}) %all-gather.8.cloned.1.call-update) | async-done | bytes 4194320 | tf_op jit(solution)/shard_map/all_gather | solution.py:12
  46.7 3.1 fusion
  49.8 124.1 %all-gather.4.cloned.1.call-done = bf16[2048,2048]{1,0:T(8,128)(2,1)} async-done(((bf16[256,2048]{1,0:T(8,128)(2,1)}), bf16[2048,2048]{1,0:T(8,128)(2,1)}) %all-gather.4.cloned.1.call-update) | async-done | bytes 8388624 | tf_op jit(solution)/shard_map/all_gather | solution.py:18
  174.0 125.8 %all-gather.6.cloned.1.call-done = bf16[2048,2048]{0,1:T(8,128)(2,1)} async-done(((bf16[256,2048]{0,1:T(8,128)(2,1)}), bf16[2048,2048]{0,1:T(8,128)(2,1)}) %all-gather.6.cloned.1.call-update) | async-done | bytes 8388624 | tf_op jit(solution)/shard_map/all_gather | solution.py:19
  299.7 25.7 %fusion.9 = bf16[1024,2048]{1,0:T(8,128)(2,1)} fusion(bf16[2048,2048]{0,1:T(8,128)(2,1)} %all-gather.6.cloned.1.call-done, bf16[2048,2048]{1,0:T(8,128)(2,1)} %all-gather.4.cloned.1.call-done, bf16[1024,2048]{1,0:T(8,128)(2,1)} %all-gather.8.cloned.1.call-done, f32[1024]{0:T(1024)S(1)} %add_rsqrt_fusion), kind=kOutput, calls=%fused_computation.8 | convolution fusion | flops 17194549248 | bytes 25169920 | tf_op jit(solution)/shard_map/tf,df->td/dot_general | solution.py:23
  325.4 0.0 reduce-scatter.2.cloned.1.call-update
  325.5 42.7 %reduce-scatter.2.cloned.1.call-done = bf16[1024,512]{1,0:T(8,128)(2,1)} async-done(((bf16[1024,2048]{1,0:T(8,128)(2,1)}), bf16[1024,512]{1,0:T(8,128)(2,1)}) %reduce-scatter.2.cloned.1.call-update) | async-done | bytes 1048592 | tf_op jit(solution)/shard_map/reduce_scatter | solution.py:24
  368.2 8.4 %copy.10 = bf16[2048,2048]{1,0:T(8,128)(2,1)} copy(bf16[2048,2048]{1,0:T(8,128)(2,1)} %all-gather.4.cloned.1.call-done) | data formatting | bytes 16777216
  376.6 8.4 %copy.11 = bf16[2048,2048]{1,0:T(8,128)(2,1)} copy(bf16[2048,2048]{1,0:T(8,128)(2,1)} %bitcast.3) | data formatting | bytes 16777216
  (1 shorter events, 0.0 us)
Async XLA Ops:
  7.2 39.6 %all-gather.8.cloned.1.call-start = ((), (), s32[]{:S(2)}) async-start(), calls=%async_computation.3 | async-start | bytes 5242880 | tf_op jit(solution)/shard_map/all_gather | solution.py:12
  7.9 166.1 %all-gather.4.cloned.1.call-start = ((), (), s32[]{:S(2)}) async-start(), calls=%async_computation.1 | async-start | bytes 9437184 | tf_op jit(solution)/shard_map/all_gather | solution.py:18
  10.7 289.0 %all-gather.6.cloned.1.call-start = ((), (), s32[]{:S(2)}) async-start(), calls=%async_computation.2 | async-start | bytes 9437184 | tf_op jit(solution)/shard_map/all_gather | solution.py:19
  13.3 354.8 %reduce-scatter.2.cloned.1.call-start = ((), (), s32[]{:S(2)}) async-start(), calls=%async_computation.4 | async-start | bytes 5242880 | tf_op jit(solution)/shard_map/reduce_scatter | solution.py:24
Sparse Core Ops, SparseCore 0:
  9.5 37.1 all-gather.7
  49.4 124.4 all-gather.3
  176.6 123.1 all-gather.5
  325.6 42.5 reduce-scatter.1
where the time goes:
time: 392 us
  waiting for transfers between devices  327 us (83%)
  matrix products  25.7 us (7%)
  local copies, waits for them, and re-layouts  19.4 us (5%)
  between operations  13.8 us (4%)
  other arithmetic  5.82 us (1%)
    all_gather x1, waiting for transfers between devices, on_device(): lax.all_gather(down_local, 'fs', axis=0, tiled=True)  126 us
    all_gather x1, waiting for transfers between devices, on_device(): lax.all_gather(up_local, 'fs', axis=0, tiled=True)  124 us
    reduce_scatter x1, waiting for transfers between devices, on_device(): lax.psum_scatter(partial_value.astype(jnp.bfloat16), 'tp', scatter_dimens...  42.7 us
    all_gather x1, waiting for transfers between devices, on_device(): gathered = lax.all_gather(tokens, 'tp', axis=1, tiled=True)  33.4 us
    dot_general x1, matrix products, on_device(): jnp.einsum('tf,df->td', hidden, down_whole, preferred_element_type=jnp.fl...  25.7 us
    unnamed x3, local copies, waits for them, and re-layouts  19.4 us
  transfers between devices with their start and end apart: 4, of which 4 were waited for; matrix products, arithmetic and copies ran while one was open for 2% of the time, Pallas kernels for 0%

commit v1 on v0

--- a/solution.py
+++ b/solution.py
@@ -9,7 +9,13 @@
 def on_device(tokens, norm_gain, up_master, down_master):
     up_local = (norm_gain[:, None] * up_master).astype(jnp.bfloat16)
     down_local = down_master.astype(jnp.bfloat16)
-    gathered = lax.all_gather(tokens, "tp", axis=1, tiled=True)
+    size = lax.axis_size("tp")
+    block, blocks = (tokens, [tokens])
+    for _ in range(size - 1):
+        block = lax.ppermute(block, "tp", [(i, (i + 1) % size) for i in range(size)])
+        blocks.insert(0, block)
+    line = jnp.concatenate(blocks, axis=1)
+    gathered = jnp.roll(line, (lax.axis_index("tp") + 1) * tokens.shape[1], axis=1)
     widened = gathered.astype(jnp.float32)
     normed = (
         widened * lax.rsqrt(jnp.mean(widened * widened, axis=-1, keepdims=True) + norm_floor)

time: 392 us -> 356 us (0.908)
  waiting for transfers between devices: 327 us -> 285 us
  local copies, waits for them, and re-layouts: 19.4 us -> 26.5 us
    all_gather x1, waiting for transfers between devices: 124 us -> 73.6 us  [on_device(): lax.all_gather(up_local, 'fs', axis=0, tiled=True)]
    ppermute x0 -> x3, waiting for transfers between devices: none -> 42.9 us  [on_device(): lax.ppermute(block, 'tp', [(i, (i + 1) % size) for i in range(size)])]
    all_gather x1 -> x0, waiting for transfers between devices: 33.4 us -> none  [on_device(): gathered = lax.all_gather(tokens, 'tp', axis=1, tiled=True)]
    unnamed x3 -> x14, local copies, waits for them, and re-layouts: 19.4 us -> 26.4 us
  transfers between devices with their start and end apart: 4 -> 6, of which waited for: 4 -> 6; matrix products, arithmetic and copies ran while one was open for 2% -> 2% of each run, Pallas kernels for 0% -> 0%
where the time goes in v1:
time: 356 us
  waiting for transfers between devices  285 us (80%)
  local copies, waits for them, and re-layouts  26.5 us (7%)
  matrix products  25.7 us (7%)
  between operations  13.8 us (4%)
  other arithmetic  3.71 us (1%)
    all_gather x1, waiting for transfers between devices, on_device(): lax.all_gather(down_local, 'fs', axis=0, tiled=True)  126 us
    all_gather x1, waiting for transfers between devices, on_device(): lax.all_gather(up_local, 'fs', axis=0, tiled=True)  73.6 us
    ppermute x3, waiting for transfers between devices, on_device(): lax.ppermute(block, 'tp', [(i, (i + 1) % size) for i in range(size)])  42.9 us
    reduce_scatter x1, waiting for transfers between devices, on_device(): lax.psum_scatter(partial_value.astype(jnp.bfloat16), 'tp', scatter_dimens...  42.7 us
    unnamed x14, local copies, waits for them, and re-layouts  26.4 us
    dot_general x1, matrix products, on_device(): jnp.einsum('tf,df->td', hidden, down_whole, preferred_element_type=jnp.fl...  25.7 us
  transfers between devices with their start and end apart: 6, of which 6 were waited for; matrix products, arithmetic and copies ran while one was open for 2% of the time, Pallas kernels for 0%

profile of v1, /device:TPU:0, one launch (start us, length us, event | category | flops | bytes accessed | tf_op | source)
XLA Modules:
  0.0 355.5 jit_solution(90454146135864159)
XLA Ops:
  7.2 0.0 copy-start
  7.2 0.0 all-gather.3.cloned.1.call-start
  7.2 2.8 multiply_convert_fusion.1
  10.0 0.0 all-gather.3.cloned.1.call-update
  10.1 0.0 all-gather.5.cloned.1.call-start
  10.1 2.5 copy.7
  12.7 0.0 all-gather.5.cloned.1.call-update
  12.7 0.0 reduce-scatter.2.cloned.1.call-start
  12.7 0.0 copy-done
  12.7 0.5 collective-permute-start
  13.3 14.4 %collective-permute-done = bf16[1024,512]{1,0:T(8,128)(2,1)S(1)} collective-permute-done((bf16[1024,512]{1,0:T(8,128)(2,1)S(1)}, bf16[1024,512]{1,0:T(8,128)(2,1)S(1)}, u32[]{:S(2)}, u32[]{:S(2)}) %collective-permute-start) | collective-permute-done | bytes 1048608 | tf_op jit(solution)/shard_map/ppermute | solution.py:15
  27.7 0.0 collective-permute-start.1
  27.7 14.2 %collective-permute-done.1 = bf16[1024,512]{1,0:T(8,128)(2,1)S(1)} collective-permute-done((bf16[1024,512]{1,0:T(8,128)(2,1)S(1)}, bf16[1024,512]{1,0:T(8,128)(2,1)S(1)}, u32[]{:S(2)}, u32[]{:S(2)}) %collective-permute-start.1) | collective-permute-done | bytes 1048608 | tf_op jit(solution)/shard_map/ppermute | solution.py:15
  41.9 0.0 collective-permute-start.2
  41.9 14.3 %collective-permute-done.2 = bf16[1024,512]{1,0:T(8,128)(2,1)} collective-permute-done((bf16[1024,512]{1,0:T(8,128)(2,1)S(1)}, bf16[1024,512]{1,0:T(8,128)(2,1)}, u32[]{:S(2)}, u32[]{:S(2)}) %collective-permute-start.2) | collective-permute-done | bytes 1048608 | tf_op jit(solution)/shard_map/ppermute | solution.py:15
  56.2 1.4 constant_dynamic-update-slice_fusion.7
  57.6 0.2 constant_dynamic-update-slice_fusion.6
  57.8 0.2 constant_dynamic-update-slice_fusion.5
  57.9 0.2 constant_dynamic-update-slice_fusion.4
  58.1 1.4 constant_dynamic-update-slice_fusion.3
  59.5 0.2 constant_dynamic-update-slice_fusion.2
  59.7 0.2 constant_dynamic-update-slice_fusion.1
  59.8 0.2 constant_dynamic-update-slice_fusion
  60.0 0.0 copy-start.1
  60.0 3.4 copy-done.1
  63.4 0.9 fusion
  64.3 73.6 %all-gather.3.cloned.1.call-done = bf16[2048,2048]{1,0:T(8,128)(2,1)} async-done(((bf16[256,2048]{1,0:T(8,128)(2,1)}), bf16[2048,2048]{1,0:T(8,128)(2,1)}) %all-gather.3.cloned.1.call-update) | async-done | bytes 8388624 | tf_op jit(solution)/shard_map/all_gather | solution.py:24
  137.9 125.8 %all-gather.5.cloned.1.call-done = bf16[2048,2048]{0,1:T(8,128)(2,1)} async-done(((bf16[256,2048]{0,1:T(8,128)(2,1)}), bf16[2048,2048]{0,1:T(8,128)(2,1)}) %all-gather.5.cloned.1.call-update) | async-done | bytes 8388624 | tf_op jit(solution)/shard_map/all_gather | solution.py:25
  263.7 25.7 %fusion.9 = bf16[1024,2048]{1,0:T(8,128)(2,1)} fusion(bf16[2048,2048]{0,1:T(8,128)(2,1)} %all-gather.5.cloned.1.call-done, bf16[2048,2048]{1,0:T(8,128)(2,1)} %all-gather.3.cloned.1.call-done, f32[1024]{0:T(1024)S(1)} %add_rsqrt_fusion, bf16[1024,4096]{1,0:T(8,128)(2,1)} %copy-done.1, s32[]{:T(128)S(6)} %select_n.14), kind=kOutput, calls=%fused_computation.8 | convolution fusion | flops 17194549248 | bytes 25169924 | tf_op jit(solution)/shard_map/tf,df->td/dot_general | solution.py:29
  289.4 0.0 reduce-scatter.2.cloned.1.call-update
  289.4 42.7 %reduce-scatter.2.cloned.1.call-done = bf16[1024,512]{1,0:T(8,128)(2,1)} async-done(((bf16[1024,2048]{1,0:T(8,128)(2,1)}), bf16[1024,512]{1,0:T(8,128)(2,1)}) %reduce-scatter.2.cloned.1.call-update) | async-done | bytes 1048592 | tf_op jit(solution)/shard_map/reduce_scatter | solution.py:30
  332.1 8.4 %copy.17 = bf16[2048,2048]{1,0:T(8,128)(2,1)} copy(bf16[2048,2048]{1,0:T(8,128)(2,1)} %all-gather.3.cloned.1.call-done) | data formatting | bytes 16777216
  340.6 8.4 %copy.18 = bf16[2048,2048]{1,0:T(8,128)(2,1)} copy(bf16[2048,2048]{1,0:T(8,128)(2,1)} %bitcast.3) | data formatting | bytes 16777216
  (1 shorter events, 0.0 us)
Async XLA Ops:
  7.2 5.6 %copy-start = (bf16[1024,512]{1,0:T(8,128)(2,1)S(1)}, bf16[1024,512]{1,0:T(8,128)(2,1)}, u32[]{:S(2)}) copy-start(bf16[1024,512]{1,0:T(8,128)(2,1)} %param.4) | copy-start | bytes 3145732
  7.2 130.7 %all-gather.3.cloned.1.call-start = ((), (), s32[]{:S(2)}) async-start(), calls=%async_computation.1 | async-start | bytes 9437184 | tf_op jit(solution)/shard_map/all_gather | solution.py:24
  10.1 253.6 %all-gather.5.cloned.1.call-start = ((), (), s32[]{:S(2)}) async-start(), calls=%async_computation.2 | async-start | bytes 9437184 | tf_op jit(solution)/shard_map/all_gather | solution.py:25
  12.7 319.4 %reduce-scatter.2.cloned.1.call-start = ((), (), s32[]{:S(2)}) async-start(), calls=%async_computation.3 | async-start | bytes 5242880 | tf_op jit(solution)/shard_map/reduce_scatter | solution.py:30
  12.7 14.9 %collective-permute-start = (bf16[1024,512]{1,0:T(8,128)(2,1)S(1)}, bf16[1024,512]{1,0:T(8,128)(2,1)S(1)}, u32[]{:S(2)}, u32[]{:S(2)}) collective-permute-start(bf16[1024,512]{1,0:T(8,128)(2,1)S(1)} %copy-done), channel_id=1, source_target_pairs={{0,1},{1,2},{2,3},{3,0},{4,5},{5,6},{6,7},{7,4},{8,9},{9,10},{10,1... | collective-permute-start | bytes 3145736 | tf_op jit(solution)/shard_map/ppermute | solution.py:15
  27.7 14.2 %collective-permute-start.1 = (bf16[1024,512]{1,0:T(8,128)(2,1)S(1)}, bf16[1024,512]{1,0:T(8,128)(2,1)S(1)}, u32[]{:S(2)}, u32[]{:S(2)}) collective-permute-start(bf16[1024,512]{1,0:T(8,128)(2,1)S(1)} %collective-permute-done), channel_id=1, source_target_pairs={{0,1},{1,2},{2,3},{3,0},{4,5},{5,6},{6,7},{7,4},{8,9},{9,10},{10,1... | collective-permute-start | bytes 3145736 | tf_op jit(solution)/shard_map/ppermute | solution.py:15
  41.9 14.3 %collective-permute-start.2 = (bf16[1024,512]{1,0:T(8,128)(2,1)S(1)}, bf16[1024,512]{1,0:T(8,128)(2,1)}, u32[]{:S(2)}, u32[]{:S(2)}) collective-permute-start(bf16[1024,512]{1,0:T(8,128)(2,1)S(1)} %collective-permute-done.1), channel_id=1, source_target_pairs={{0,1},{1,2},{2,3},{3,0},{4,5},{5,6},{6,7},{7,4},{8,9},{9,10},{10,1... | collective-permute-start | bytes 3145736 | tf_op jit(solution)/shard_map/ppermute | solution.py:15
  60.0 3.4 copy-start.1
Sparse Core Ops, SparseCore 0:
  10.7 127.1 all-gather.2
  140.5 123.1 all-gather.4
  289.5 42.5 reduce-scatter.1
